TPU v7x, 32 devices: a whole 2x2x4 slice. The times are simulated.
32 devices in a mesh: grp: 2 (over y), sp: 4 (over z), tp: 4 (over x, core).
Axes of the slice: x: 2, y: 2, z: 4, core: 2. Of those that a mesh axis runs over, the one named last changes fastest.
Arguments:
- resid: bfloat16 [4096, 2048], P(('grp', 'sp', 'tp')), parts along dimension 0, may hold values from -6 to 6
- pool_input: bfloat16 [4096, 512], P(('grp', 'sp'), 'tp'), parts along dimension 0, may hold values from -6 to 6
- group_map: bfloat16 [4, 128, 128], P('tp'), may hold values from -0.5 to 0.5
- pool_scale: bfloat16 [512], P('tp'), may hold values from 0.099609375 to 1.8984375
- out_proj: bfloat16 [512, 2048], P('tp'), may hold values from -0.25 to 0.25
- norm_gain: bfloat16 [2048], replicated, may hold values from 0.099609375 to 1.8984375
- routes: int32 [4096, 2], P(('grp', 'sp', 'tp')), parts along dimension 0, may hold values from 0 to 3, all different within a row; in each aligned block of 128 rows (0 to 127, 128 to 255, ...) at most 80 rows name the same one
- route_weight: float32 [4096, 2], P(('grp', 'sp', 'tp')), parts along dimension 0, may hold values from 0.2 to 1
- expert_gate: bfloat16 [4, 2048, 3584], P('sp', None, 'tp'), may hold values from -0.125 to 0.125
- expert_up: bfloat16 [4, 2048, 3584], P('sp', None, 'tp'), may hold values from -0.125 to 0.125
- expert_down: bfloat16 [4, 3584, 2048], P('sp', 'tp'), may hold values from -0.09375 to 0.09375
Outputs:
- layer_out: bfloat16 [4096, 2048], P(('grp', 'sp', 'tp')), parts along dimension 0
There are 2 independent parts, one for each index of `grp`. A program takes and returns all parts, laid end to end along the dimension named above; an argument that names none is the same for every part. Nothing has to cross between parts.
Inputs may be any that keep to these rules, and one draw needn't show every extreme that they name: The 2 routes of a token differ. Among the tokens of one device (aligned blocks of 128 tokens), no expert is named more than 80 times, and in every draw some device names some expert exactly 80 times.
All inputs are finite; a program needn't handle non-finite values.
Results may differ from a plain program's by a relative error of at most 0.011.
Values may be sent and summed in bfloat16 or wider, within the bound.
A program may use at most 128 MiB of HBM per device.

v0:
```python
import jax
import jax.numpy as jnp
from jax import lax
from jax.sharding import PartitionSpec as P

GROUPS = 4


norm_eps = 1e-06


def from_behind(value, axis, steps):
    count = lax.axis_size(axis)
    leading, last = (max(0, -steps), min(count, count - steps))
    return lax.ppermute(value, axis, [(source, source + steps) for source in range(leading, last)])


def expert_block(arrived, gate_w, up_w, down_w):
    width = arrived.shape[-1]
    flat = arrived.reshape(-1, width)
    gate = jnp.dot(flat, gate_w, preferred_element_type=jnp.float32)
    up_value = jnp.dot(flat, up_w, preferred_element_type=jnp.float32)
    hidden = (jax.nn.silu(gate) * up_value).astype(jnp.bfloat16)
    partial_out = jnp.dot(hidden, down_w, preferred_element_type=jnp.float32).astype(jnp.bfloat16)
    return partial_out.reshape(arrived.shape)


def local(
    resid,
    pool_input,
    group_map,
    pool_scale,
    out_proj,
    norm_gain,
    routes,
    route_weight,
    expert_gate,
    expert_up,
    expert_down,
):
    seq_rows = pool_input.shape[0]
    local_groups = group_map.shape[0]
    group_dim = group_map.shape[1]
    reach = 2**GROUPS - 1
    rim_rows = from_behind(pool_input[seq_rows - reach :], "sp", 1)
    extended = jnp.concatenate([rim_rows, pool_input], axis=0).astype(jnp.float32)
    positions = lax.axis_index("sp") * seq_rows + jnp.arange(1, seq_rows + 1, dtype=jnp.int32)
    group = lax.axis_index("tp") * local_groups + 0
    window = jnp.left_shift(jnp.int32(2), group)
    window_sum = jnp.zeros((seq_rows, group_dim), jnp.float32)
    for back in range(reach + 1):
        window_sum = window_sum + jnp.where(
            back < window, extended[reach - back : reach - back + seq_rows], jnp.float32(0.0)
        )
    divisor = jnp.minimum(positions, window).astype(jnp.float32)
    pooled = (window_sum / divisor[:, None] - extended[reach:]).astype(jnp.bfloat16)
    product = jnp.dot(pooled, group_map[0], preferred_element_type=jnp.float32)
    scale = pool_scale.astype(jnp.float32)
    pieces = (product * scale).astype(jnp.bfloat16)
    own_rows = resid.shape[0]
    width = resid.shape[1]
    mix = lax.psum_scatter(
        jnp.dot(pieces, out_proj, preferred_element_type=jnp.float32),
        "tp",
        scatter_dimension=0,
        tiled=True,
    )
    mixed = (resid.astype(jnp.float32) + mix).astype(jnp.bfloat16)
    residual = mixed.astype(jnp.float32)
    scaled = residual * lax.rsqrt(jnp.mean(residual * residual, axis=1, keepdims=True) + norm_eps)
    normed = (scaled * norm_gain.astype(jnp.float32)).astype(jnp.bfloat16)
    top_count = routes.shape[1]
    lanes = lax.axis_size("tp")
    seq_devices = lax.axis_size("sp")
    experts = seq_devices * expert_gate.shape[0]
    slots = max(2, 5 * own_rows * top_count // (4 * experts))
    flat_routes = routes.reshape(-1)
    onehot = (flat_routes[:, None] == jnp.arange(experts, dtype=jnp.int32)[None, :]).astype(
        jnp.int32
    )
    ranks = jnp.cumsum(onehot, axis=0) - onehot
    slot_of = jnp.sum(ranks * onehot, axis=1)
    target = flat_routes * slots + slot_of
    placing = (jnp.arange(experts * slots, dtype=jnp.int32)[:, None] == target[None, :]).astype(
        jnp.bfloat16
    )
    repeated = jnp.repeat(normed, top_count, axis=0)
    send_rows = jnp.dot(placing, repeated, preferred_element_type=jnp.float32).astype(jnp.bfloat16)
    gate_w = expert_gate[0]
    up_w = expert_up[0]
    down_w = expert_down[0]
    everyone = lax.all_gather(
        lax.all_to_all(
            send_rows.reshape(experts, slots, width), "sp", split_axis=0, concat_axis=0, tiled=True
        )[:, None],
        "tp",
        axis=1,
        tiled=True,
    )
    partials = expert_block(
        everyone.reshape(-1, everyone.shape[2], everyone.shape[3]), gate_w, up_w, down_w
    )
    returned = lax.all_to_all(partials, ("sp", "tp"), split_axis=0, concat_axis=0, tiled=True)
    summed = jnp.sum(
        returned.reshape(experts, lanes, slots, width).astype(jnp.float32), axis=1
    ).reshape(experts * slots, width)
    picked = jnp.take(summed, target, axis=0).reshape(own_rows, top_count, width)
    moe = jnp.sum(picked * route_weight[:, :, None], axis=1)
    return (residual + moe).astype(jnp.bfloat16)


def solution(mesh):
    return jax.shard_map(
        local,
        mesh=mesh,
        in_specs=(
            P(("grp", "sp", "tp"), None),
            P(("grp", "sp"), "tp"),
            P("tp", None, None),
            P("tp"),
            P("tp", None),
            P(),
            P(("grp", "sp", "tp"), None),
            P(("grp", "sp", "tp"), None),
            P("sp", None, "tp"),
            P("sp", None, "tp"),
            P("sp", "tp", None),
        ),
        out_specs=P(("grp", "sp", "tp"), None),
        check_vma=False,
    )
```

profile of v0, /device:TPU:11, one launch (start us, length us, event | category | flops | bytes accessed | tf_op | source)
XLA Modules:
  0.0 311.2 jit_solution(17974632546630839464)
XLA Ops:
  6.5 0.7 slice.58
  7.3 3.2 %collective-permute-start = (bf16[15,128]{1,0:T(8,128)(2,1)S(1)}, bf16[15,128]{1,0:T(8,128)(2,1)S(1)}, u32[]{:S(2)}, u32[]{:S(2)}) collective-permute-start(bf16[15,128]{1,0:T(8,128)(2,1)S(1)} %slice.58), channel_id=1, source_target_pairs={{0,4},{4,8},{8,12},{1,5},{5,9},{9,13},{2,6},{6,10},{10,14},{3,7},{... | collective-permute-start | bytes 11528 | tf_op jit(solution)/shard_map/ppermute | solution.py:15
  10.5 0.7 convert_element_type.64
  11.2 0.4 collective-permute-done
  11.6 0.9 maximum_convert_fusion
  12.6 3.9 %fusion.5 = f32[512,2048]{1,0:T(8,128)} fusion(bf16[128,2048]{1,0:T(8,128)(2,1)S(1)} %copy-done, f32[527,128]{1,0:T(8,128)S(1)} %maximum_convert_fusion, f32[128]{0:T(128)S(1)} %convert_element_type.64, f32[512]{0:T(512)S(1)} %minimum_convert_fusion, pred[]{:T(512)S(6)} %gt.63, pred[]{:T(512)S(6)} %gt.62, pred[]{:T(512)S(6)} %gt.61, pred[]{:T(512)S(6)} %gt.60, ...), kind=kOutput, calls=%fused_computation.15 | convolution fusion | flops 287571968 | bytes 8948240 | tf_op jit(solution)/shard_map/dot_general | solution.py:63
  16.6 0.6 copy-done.4
  17.3 0.1 eq.39
  17.4 0.1 reshape.103
  17.6 1.2 reduce-window.6
  19.3 43.2 %reduce-scatter.2.cloned.1.call-done = f32[128,2048]{1,0:T(8,128)} async-done(((f32[512,2048]{1,0:T(8,128)}), f32[128,2048]{1,0:T(8,128)}) %reduce-scatter.2.cloned.1.call-update) | async-done | bytes 1048592 | tf_op jit(solution)/shard_map/reduce_scatter | solution.py:62
  62.5 1.5 fusion.6
  64.0 0.8 copy-done.1
  64.8 0.2 fusion.8
  64.9 0.6 broadcast_in_dim.45
  65.6 0.4 reshape.105
  66.0 0.5 convolution_convert_fusion.1
  66.5 33.0 %all_to_all.10 = bf16[4,80,2048]{2,1,0:T(8,128)(2,1)} all-to-all(bf16[4,80,2048]{2,1,0:T(8,128)(2,1)S(1)} %bitcast.56), channel_id=1, replica_groups=mesh['grp'=2,'sp'=4,'tp'=4] {'sp'}, dimensions={0} | all-to-all | bytes 2621440 | tf_op jit(solution)/shard_map/all_to_all | solution.py:93
  99.5 42.0 %all-gather.3.cloned.1.call-done = bf16[4,320,2048]{2,1,0:T(8,128)(2,1)} async-done(((bf16[4,80,2048]{2,1,0:T(8,128)(2,1)}), bf16[4,320,2048]{2,1,0:T(8,128)(2,1)}) %all-gather.3.cloned.1.call-update) | async-done | bytes 5242896 | tf_op jit(solution)/shard_map/all_gather | solution.py:92
  141.5 10.0 %fusion.2 = f32[1280,896]{1,0:T(8,128)} fusion(bf16[1280,2048]{1,0:T(8,128)(2,1)} %bitcast.60, bf16[1,2048,896]{2,1,0:T(8,128)(2,1)} %param.19), kind=kOutput, calls=%fused_computation.6 | convolution fusion | flops 4697620480 | bytes 13500416 | tf_op jit(solution)/shard_map/dot_general | solution.py:21
  151.5 17.6 %convolution_convert_fusion = bf16[1280,2048]{1,0:T(8,128)(2,1)} fusion(bf16[1,896,2048]{2,1,0:T(8,128)(2,1)} %param.21, f32[1280,896]{1,0:T(8,128)} %fusion.2, bf16[1280,2048]{1,0:T(8,128)(2,1)} %bitcast.61, bf16[1,2048,896]{2,1,0:T(8,128)(2,1)} %param.20), kind=kOutput, calls=%fused_computation.2 | convolution fusion | flops 9404743680 | bytes 22413312 | tf_op jit(solution)/shard_map/dot_general | solution.py:24
  169.1 6.1 %all-to-all-start.1 = ((bf16[16,80,2048]{2,1,0:T(8,128)(2,1)}), bf16[16,80,2048]{2,1,0:T(8,128)(2,1)}, u32[]{:S(2)}, u32[]{:S(2)}) async-start(bf16[16,80,2048]{2,1,0:T(8,128)(2,1)} %bitcast.55), calls=%async_computation.2 | async-start | bytes 10485760 | tf_op jit(solution)/shard_map/all_to_all | solution.py:103
  175.1 0.1 reduce_sum.41
  175.3 0.1 copy.28
  175.4 0.1 mul.90
  175.6 0.1 copy.27
  175.9 114.2 %all-to-all-done.1 = bf16[16,80,2048]{2,1,0:T(8,128)(2,1)} async-done(((bf16[16,80,2048]{2,1,0:T(8,128)(2,1)}), bf16[16,80,2048]{2,1,0:T(8,128)(2,1)}, u32[]{:S(2)}, u32[]{:S(2)}) %all-to-all-start.1) | async-done | bytes 5242912 | tf_op jit(solution)/shard_map/all_to_all | solution.py:103
  290.1 3.9 %convert_reduce_fusion = f32[4,80,2048]{2,1,0:T(8,128)S(1)} fusion(bf16[16,80,2048]{2,1,0:T(8,128)(2,1)} %all-to-all-done.1), kind=kLoop, calls=%fused_computation.1 | loop fusion | flops 4587520 | bytes 7864320 | tf_op jit(solution)/shard_map/reduce_sum | solution.py:104
  294.0 2.7 gather_fusion
  296.7 2.5 gather.7
  299.2 4.2 %multiply_reduce_fusion = f32[128,2048]{1,0:T(8,128)S(1)} fusion(f32[128,2,2048]{2,1,0:T(2,128)S(1)} %gather.7, pred[128,2]{1,0:T(8,128)(4,1)S(1)} %copy.27, f32[128,2]{1,0:T(8,128)S(1)} %copy.29), kind=kLoop, calls=%fused_computation.9 | loop fusion | flops 1310720 | bytes 3147008 | tf_op jit(solution)/shard_map/reduce_sum | solution.py:108
  303.5 0.9 fusion.9
  (35 shorter events, 0.9 us)
Async XLA Ops:
  6.5 6.0 %copy-start = (bf16[128,2048]{1,0:T(8,128)(2,1)S(1)}, bf16[128,2048]{1,0:T(8,128)(2,1)}, u32[]{:S(2)}) copy-start(bf16[128,2048]{1,0:T(8,128)(2,1)} %param.15) | copy-start | bytes 1572868
  6.5 55.9 %reduce-scatter.2.cloned.1.call-start = ((), (), s32[]{:S(2)}) async-start(), calls=%async_computation.3 | async-start | bytes 5242880 | tf_op jit(solution)/shard_map/reduce_scatter | solution.py:62
  7.3 4.3 %collective-permute-start = (bf16[15,128]{1,0:T(8,128)(2,1)S(1)}, bf16[15,128]{1,0:T(8,128)(2,1)S(1)}, u32[]{:S(2)}, u32[]{:S(2)}) collective-permute-start(bf16[15,128]{1,0:T(8,128)(2,1)S(1)} %slice.58), channel_id=1, source_target_pairs={{0,4},{4,8},{8,12},{1,5},{5,9},{9,13},{2,6},{6,10},{10,14},{3,7},{... | collective-permute-start | bytes 11528 | tf_op jit(solution)/shard_map/ppermute | solution.py:15
  16.5 0.7 copy-start.4
  16.5 1.1 copy-start.5
  16.5 46.0 %copy-start.3 = (bf16[128,2048]{1,0:T(8,128)(2,1)S(1)}, bf16[128,2048]{1,0:T(8,128)(2,1)}, u32[]{:S(2)}) copy-start(bf16[128,2048]{1,0:T(8,128)(2,1)} %param.11) | copy-start | bytes 1572868
  16.5 125.0 %all-gather.3.cloned.1.call-start = ((), (), s32[]{:S(2)}) async-start(), calls=%async_computation.4 | async-start | bytes 6553600 | tf_op jit(solution)/shard_map/all_gather | solution.py:92
  64.0 0.8 copy-start.1
  169.1 6.7 %copy-start.6 = (f32[128,2]{0,1:T(2,128)S(1)}, f32[128,2]{0,1:T(2,128)}, u32[]{:S(2)}) copy-start(f32[128,2]{0,1:T(2,128)} %param.18) | copy-start | bytes 3076
  169.1 121.0 %all-to-all-start.1 = ((bf16[16,80,2048]{2,1,0:T(8,128)(2,1)}), bf16[16,80,2048]{2,1,0:T(8,128)(2,1)}, u32[]{:S(2)}, u32[]{:S(2)}) async-start(bf16[16,80,2048]{2,1,0:T(8,128)(2,1)} %bitcast.55), calls=%async_computation.2 | async-start | bytes 10485760 | tf_op jit(solution)/shard_map/all_to_all | solution.py:103
  296.7 6.8 %copy-start.2 = (bf16[128,2048]{1,0:T(8,128)(2,1)S(1)}, bf16[128,2048]{1,0:T(8,128)(2,1)}, u32[]{:S(2)}) copy-start(bf16[128,2048]{1,0:T(8,128)(2,1)} %copy-done.1) | copy-start | bytes 1572868
Sparse Core Ops, SparseCore 0:
  16.7 45.7 reduce-scatter.1
  99.7 41.8 all-gather.2
where the time goes:
time: 312 us; the launch traced here: 311 us
  waiting for transfers between devices  200 us (64%)
  blocking collectives  33 us (11%)
  matrix products  32 us (10%)
  other arithmetic  13.7 us (4%)
  between operations  13.6 us (4%)
  local copies, waits for them, and re-layouts  9.83 us (3%)
  starting transfers between devices  9.3 us (3%)
    all_to_all x1, waiting for transfers between devices, local(): lax.all_to_all(partials, ('sp', 'tp'), split_axis=0, concat_axis=0, tiled...  114 us
    reduce_scatter x1, waiting for transfers between devices, local(): lax.psum_scatter(jnp.dot(pieces, out_proj, preferred_element_type=jnp.flo...  43.2 us
    all_gather x1, waiting for transfers between devices, local(): lax.all_gather(lax.all_to_all(send_rows.reshape(experts, slots, width), '...  42 us
    all_to_all x1, blocking collectives, local(): lax.all_to_all(send_rows.reshape(experts, slots, width), 'sp', split_axis...  33 us
    dot_general x1, matrix products, expert_block(): jnp.dot(hidden, down_w, preferred_element_type=jnp.float32)  17.6 us
    dot_general x1, matrix products, expert_block(): gate = jnp.dot(flat, gate_w, preferred_element_type=jnp.float32)  9.98 us
  transfers between devices with their start and end apart: 4, of which 4 were waited for; matrix products, arithmetic and copies ran while one was open for 1% of the time, Pallas kernels for 0%

commit v1 on v0

v1 whole, which is shorter than its diff:
```python
import functools

import jax
import jax.numpy as jnp
from jax import lax
from jax.experimental import pallas as pl
from jax.experimental.pallas import tpu as pltpu
from jax.sharding import PartitionSpec as P

GROUPS = 4
norm_eps = 1e-06
BF = jnp.bfloat16
F32 = jnp.float32
MESH = pl.DeviceIdType.MESH
RIM = 2**GROUPS


def offset(j):
    half = (j + 1) // 2
    return half * (2 * lax.rem(j, 2) - 1)


def kernel(
    S, T, R, SL,
    resid, pool, gmap, scale, oproj, gain, routes, routes_t, weight, wg, wu, wd,
    out,
    wgu_v, wd_v, opj, rim, piece, gout, stage, inbox, pbuf, rbuf, fbuf, fin, ret,
    acc, hid, mixed_v, normed_v,
    w_sem, o_far_s, o_far_r, o_near_s, o_near_r, rim_s, rim_r, pc_s, pc_r,
    z_s, z_r, f_s, f_r, n_s, n_r, pn_s, pn_r, pf_s, pf_r, rz_s, rz_r,
):
    s = lax.axis_index("sp")
    t = lax.axis_index("tp")
    H = T // 2
    D = resid.shape[1]
    F = wd.shape[0]
    near = t + 1 - 2 * lax.rem(t, 2)

    def up(k):
        return lax.rem(t + 2 * k, T)

    def down(base, k):
        return lax.rem(base - 2 * k + 2 * T, T)

    def remote(src, dst, ss, rs, sp=None, tp=None):
        return pltpu.make_async_remote_copy(
            src_ref=src, dst_ref=dst, send_sem=ss, recv_sem=rs,
            device_id={"sp": s if sp is None else sp, "tp": t if tp is None else tp},
            device_id_type=MESH,
        )

    loads = [
        pltpu.make_async_copy(wg, wgu_v.at[:, pl.ds(0, F)], w_sem.at[0]),
        pltpu.make_async_copy(wu, wgu_v.at[:, pl.ds(F, F)], w_sem.at[1]),
        pltpu.make_async_copy(wd, wd_v, w_sem.at[2]),
    ]
    for load in loads:
        load.start()

    barrier = pltpu.get_barrier_semaphore()

    @pl.loop(1, S)
    def _(j):
        pl.semaphore_signal(
            barrier, inc=1, device_id={"sp": lax.rem(s + j, S), "tp": t}, device_id_type=MESH
        )

    for j in range(1, T):
        pl.semaphore_signal(
            barrier, inc=1, device_id={"sp": s, "tp": lax.rem(t + j, T)}, device_id_type=MESH
        )
    pl.semaphore_wait(barrier, S - 1 + T - 1)

    seq = pool.shape[0]
    rim_copy = remote(
        pool.at[pl.ds(seq - RIM, RIM)], rim, rim_s.at[0], rim_r.at[0], sp=lax.rem(s + 1, S)
    )
    rim_copy.start()

    def o_far(k):
        return remote(oproj, opj.at[t], o_far_s.at[k], o_far_r.at[k], tp=up(k))

    def o_near(k):
        block = down(t, k)
        return remote(
            oproj if k == 0 else opj.at[block], opj.at[block], o_near_s.at[k], o_near_r.at[k],
            tp=near,
        )

    for k in range(1, H):
        o_far(k).start()
    o_near(0).start()

    E = S
    EP = max(8, E)
    e_row = lax.broadcasted_iota(jnp.int32, (EP, R), 0)
    hot_row = [e_row == routes_t[k : k + 1, :] for k in range(2)]
    both_row = jnp.where(hot_row[0] | hot_row[1], 1.0, 0.0).astype(BF)
    before = lax.broadcasted_iota(jnp.int32, (R, R), 0) < lax.broadcasted_iota(
        jnp.int32, (R, R), 1
    )
    rank_row = jnp.dot(both_row, jnp.where(before, 1.0, 0.0).astype(BF), preferred_element_type=F32)
    slot_row = rank_row + (e_row * SL).astype(F32)
    tgt_row = [jnp.sum(jnp.where(h, slot_row, 0.0), axis=0, keepdims=True) for h in hot_row]

    EL = 128
    e_col = lax.broadcasted_iota(jnp.int32, (R, EL), 1)
    hot_col = [e_col == routes[:, k : k + 1] for k in range(2)]
    both_col = jnp.where(hot_col[0] | hot_col[1], 1.0, 0.0).astype(BF)
    after = lax.broadcasted_iota(jnp.int32, (R, R), 1) < lax.broadcasted_iota(
        jnp.int32, (R, R), 0
    )
    rank_col = jnp.dot(jnp.where(after, 1.0, 0.0).astype(BF), both_col, preferred_element_type=F32)
    slot_col = rank_col + (e_col * SL).astype(F32)
    tgt_col = [jnp.sum(jnp.where(h, slot_col, 0.0), axis=1, keepdims=True) for h in hot_col]

    rim_copy.wait_recv()
    values = pool[...].astype(F32)
    rim_v = jnp.where(s > 0, rim[...].astype(F32), 0.0)
    run = jnp.concatenate([rim_v, values], axis=0)
    window_sum = None
    for g in range(GROUPS):
        run = run + pltpu.roll(run, 2**g, 0)
        part = run[RIM:]
        window_sum = part if g == 0 else jnp.where(t >= g, part, window_sum)
    window = jnp.int32(2)
    for g in range(1, GROUPS):
        window = jnp.where(t >= g, jnp.int32(2 ** (g + 1)), window)
    position = s * seq + 1 + lax.broadcasted_iota(jnp.int32, (seq, 128), 0)
    divisor = jnp.minimum(position, window).astype(F32)
    pooled = (window_sum / divisor - values).astype(BF)
    product = jnp.dot(pooled, gmap[0], preferred_element_type=F32)
    piece[...] = (product * scale[...].astype(F32)).astype(BF).reshape(T, R, 128)

    def piece_copy(j):
        q = lax.rem(t + j, T)
        return remote(piece.at[q], gout.at[t], pc_s.at[j], pc_r.at[j], tp=q)

    for j in range(1, T):
        piece_copy(j).start()

    for k in range(1, H):
        o_far(k).wait_recv()
        o_near(k).start()

    for j in range(1, T):
        piece_copy(j).wait_recv()
    for k in range(H):
        o_near(k).wait_recv()

    gout[t] = piece[t]
    opj[t] = oproj[...]
    mix = resid[...].astype(F32)
    total = jnp.dot(gout[0], opj[0], preferred_element_type=F32)
    for q in range(1, T):
        total = total + jnp.dot(gout[q], opj[q], preferred_element_type=F32)
    mixed = (mix + total).astype(BF)
    mixed_v[...] = mixed
    residual = mixed.astype(F32)
    scaled = residual * lax.rsqrt(jnp.mean(residual * residual, axis=1, keepdims=True) + norm_eps)
    normed_v[...] = (scaled * gain[...].astype(F32)).astype(BF)

    slot_iota = lax.broadcasted_iota(jnp.int32, (SL, R), 0)

    def rows_of(e):
        want = (slot_iota + e * SL).astype(F32)
        place = jnp.where((tgt_row[0] == want) | (tgt_row[1] == want), 1.0, 0.0).astype(BF)
        return jnp.dot(place, normed_v[...], preferred_element_type=F32).astype(BF)

    def dest(j):
        return lax.rem(s + offset(j) + S, S)

    def source(j):
        return lax.rem(s - offset(j) + S, S)

    def z_copy(j):
        return remote(stage.at[j], inbox.at[s, t], z_s.at[j], z_r.at[j], sp=dest(j))

    def far_copy(j, k):
        block = inbox.at[source(j), t]
        return remote(block, block, f_s.at[j, k], f_r.at[j, k], tp=up(k))

    def near_copy(j, k):
        block = inbox.at[source(j), down(t, k)]
        return remote(block, block, n_s.at[j, k], n_r.at[j, k], tp=near)

    def forward_own(j):
        for k in range(1, H):
            far_copy(j, k).start()
        near_copy(j, 0).start()

    def p_near(j, k):
        return remote(
            pbuf.at[j, down(near, k)], rbuf.at[j, k], pn_s.at[j, k], pn_r.at[j, k], tp=near
        )

    def p_far(j, k):
        q = down(t, k)
        return remote(pbuf.at[j, q], fbuf.at[j, k], pf_s.at[j, k], pf_r.at[j, k], tp=q)

    def back(j):
        return remote(fin.at[j], ret.at[s], rz_s.at[j], rz_r.at[j], sp=source(j))

    inbox[s, t] = rows_of(s)
    forward_own(0)

    @pl.loop(1, S)
    def _(j):
        stage[j] = rows_of(dest(j))
        z_copy(j).start()

    for load in loads:
        load.wait()

    def arrive(j):
        z_copy(j).wait_recv()
        forward_own(j)

    if S > 1:
        arrive(1)

    NT = 256 if (2 * F) % 256 == 0 else 128
    DT = 256 if D % 256 == 0 else 128

    @pl.loop(0, S + 2)
    def _(j):
        @pl.when(j + 2 < S)
        def _():
            arrive(j + 2)

        @pl.when((j >= 1) & (j <= S))
        def _():
            i = j - 1
            for k in range(H):
                p_near(i, k).wait_recv()
            for k in range(1, H):
                q = down(t, k)
                pbuf[i, q] = (pbuf[i, q].astype(F32) + rbuf[i, k].astype(F32)).astype(BF)
                p_far(i, k).start()

        @pl.when(j < S)
        def _():
            for k in range(1, H):
                far_copy(j, k).wait_recv()
                near_copy(j, k).start()

        @pl.when(j >= 2)
        def _():
            i = j - 2
            value = pbuf[i, t].astype(F32) + rbuf[i, 0].astype(F32)
            for k in range(1, H):
                p_far(i, k).wait_recv()
                value = value + fbuf[i, k].astype(F32)
            fin[i] = value.astype(BF)

            @pl.when(i > 0)
            def _():
                back(i).start()

        @pl.when(j < S)
        def _():
            for k in range(H):
                near_copy(j, k).wait_recv()
            src = source(j)

            @pl.loop(0, 2 * F // NT)
            def _(n):
                cols = pl.ds(pl.multiple_of(n * NT, NT), NT)
                x = inbox[src].reshape(T * SL, D)
                acc[:, cols] = jnp.dot(x, wgu_v[:, cols], preferred_element_type=F32)

            gate = acc[:, :F]
            hid[...] = (gate / (1.0 + jnp.exp(-gate)) * acc[:, F:]).astype(BF)

            @pl.loop(0, D // DT)
            def _(n):
                cols = pl.ds(pl.multiple_of(n * DT, DT), DT)
                y = jnp.dot(hid[...], wd_v[:, cols], preferred_element_type=F32)
                pbuf[j, :, :, cols] = y.astype(BF).reshape(T, SL, DT)

            for k in range(H):
                p_near(j, k).start()

    @pl.loop(1, S)
    def _(j):
        back(j).wait_recv()

    ret[s] = fin[0]
    flat = ret[...].reshape(S * SL, D)
    lanes = lax.broadcasted_iota(jnp.int32, (R, S * SL), 1).astype(F32)
    total = mixed_v[...].astype(F32)
    picked = [
        weight[:, k : k + 1]
        * jnp.dot(
            jnp.where(tgt_col[k] == lanes, 1.0, 0.0).astype(BF), flat, preferred_element_type=F32
        )
        for k in range(2)
    ]
    out[...] = (total + (picked[0] + picked[1])).astype(BF)

    rim_copy.wait_send()
    for k in range(1, H):
        o_far(k).wait_send()
    for k in range(H):
        o_near(k).wait_send()
    for j in range(1, T):
        piece_copy(j).wait_send()

    @pl.loop(0, S)
    def _(j):
        for k in range(1, H):
            far_copy(j, k).wait_send()
            p_far(j, k).wait_send()
        for k in range(H):
            near_copy(j, k).wait_send()
            p_near(j, k).wait_send()

    @pl.loop(1, S)
    def _(j):
        z_copy(j).wait_send()
        back(j).wait_send()


def local(
    resid, pool_input, group_map, pool_scale, out_proj, norm_gain, routes, route_weight,
    expert_gate, expert_up, expert_down,
):
    S, T = lax.axis_size("sp"), lax.axis_size("tp")
    R, D = resid.shape
    H = T // 2
    top = routes.shape[1]
    experts = S * expert_gate.shape[0]
    slots = max(2, 5 * R * top // (4 * experts))
    SL = -(-slots // 16) * 16
    F = expert_down.shape[1]
    GD = group_map.shape[1]
    vmem, hbm = pl.BlockSpec(memory_space=pltpu.VMEM), pl.BlockSpec(memory_space=pl.ANY)
    dma = lambda *n: pltpu.SemaphoreType.DMA(n)
    buf = lambda *n: pltpu.VMEM(n, BF)
    return pl.pallas_call(
        functools.partial(kernel, S, T, R, SL),
        out_shape=jax.ShapeDtypeStruct((R, D), BF),
        in_specs=[vmem] * 9 + [hbm] * 3,
        out_specs=vmem,
        scratch_shapes=[
            buf(D, 2 * F), buf(F, D), buf(T, GD, D), buf(RIM, GD), buf(T, R, GD), buf(T, R, GD),
            buf(S, SL, D), buf(S, T, SL, D), buf(S, T, SL, D), buf(S, H, SL, D), buf(S, H, SL, D),
            buf(S, SL, D), buf(S, SL, D),
            pltpu.VMEM((T * SL, 2 * F), F32), buf(T * SL, F), buf(R, D), buf(R, D),
            dma(3), dma(H), dma(H), dma(H), dma(H), dma(1), dma(1), dma(T), dma(T),
            dma(S), dma(S), dma(S, H), dma(S, H), dma(S, H), dma(S, H),
            dma(S, H), dma(S, H), dma(S, H), dma(S, H), dma(S), dma(S),
        ],
        compiler_params=pltpu.CompilerParams(
            collective_id=0, has_side_effects=True, vmem_limit_bytes=63 * 1024 * 1024
        ),
    )(
        resid, pool_input, group_map, pool_scale.reshape(1, -1), out_proj,
        norm_gain.reshape(1, -1), routes, routes.T, route_weight,
        expert_gate[0], expert_up[0], expert_down[0],
    )


def solution(mesh):
    return jax.shard_map(
        local,
        mesh=mesh,
        in_specs=(
            P(("grp", "sp", "tp"), None),
            P(("grp", "sp"), "tp"),
            P("tp", None, None),
            P("tp"),
            P("tp", None),
            P(),
            P(("grp", "sp", "tp"), None),
            P(("grp", "sp", "tp"), None),
            P("sp", None, "tp"),
            P("sp", None, "tp"),
            P("sp", "tp", None),
        ),
        out_specs=P(("grp", "sp", "tp"), None),
        check_vma=False,
    )
```

time: 312 us -> 120 us (0.38)
  the two profiles are of different devices: /device:TPU:11 before, /device:TPU:0 now
where the time goes in v1:
time: 120 us
  Pallas kernels  114 us (95%)
  local copies, waits for them, and re-layouts  5.98 us (5%)
    pallas_call x1, Pallas kernels, local(): pl.pallas_call(functools.partial(kernel, S, T, R, SL), out_shape=jax.Shap...  114 us
    unnamed x3, local copies, waits for them, and re-layouts  4.7 us

profile of v1, /device:TPU:0, one launch (start us, length us, event | category | flops | bytes accessed | tf_op | source)
XLA Modules:
  0.0 119.7 jit_solution(2020681668324460667)
XLA Ops:
  0.0 1.3 %reshape.7.gain = bf16[1,2048]{1,0:T(2,128)(2,1)} reshape(bf16[2048]{0:T(1024)(128)(2,1)} %param.16) | data formatting | bytes 8192 | tf_op jit(solution)/shard_map/reshape | solution.py:359
  1.3 1.4 %copy.13.weight = f32[128,2]{1,0:T(8,128)} copy(f32[128,2]{0,1:T(2,128)} %param.18) | data formatting | bytes 2048 | tf_op args[7]
  2.7 1.4 %copy.12.routes = s32[128,2]{1,0:T(8,128)} copy(s32[128,2]{0,1:T(2,128)} %param.17) | data formatting | bytes 2048 | tf_op args[6]
  4.1 113.7 %shard_map.109 = bf16[128,2048]{1,0:T(8,128)(2,1)} custom-call(bf16[128,2048]{1,0:T(8,128)(2,1)} %resid.1, bf16[512,128]{1,0:T(8,128)(2,1)} %pool.1, bf16[1,128,128]{2,1,0:T(8,128)(2,1)} %gmap.1, bf16[1,128]{1,0:T(2,128)(2,1)} %bitcast.9, bf16[128,2048]{1,0:T(8,128)(2,1)} %oproj.1, bf16[1,2048]{1,0:T(2,128)(2,1)} %reshape.7.gain, s32[128,2]{1,0:T(8,128)} %copy.12.routes, ...), custom_call_target="tpu_custom_call" | custom-call | tf_op jit(solution)/shard_map/pallas_call | solution.py:340
  117.8 1.9 %copy.15 = bf16[128,2048]{1,0:T(8,128)(2,1)} copy(bf16[128,2048]{1,0:T(8,128)(2,1)} %shard_map.109) | data formatting | bytes 1048576

commit v2 on v1

--- a/solution.py
+++ b/solution.py
@@ -15,14 +15,17 @@
 RIM = 2**GROUPS
 
 
-def offset(j):
+def nearest(s, j, S):
+    low = jnp.minimum(s, S - 1 - s)
     half = (j + 1) // 2
-    return half * (2 * lax.rem(j, 2) - 1)
+    both = half * (2 * lax.rem(j, 2) - 1)
+    rest = (j - low) * (1 - 2 * ((2 * s) // S))
+    return s + jnp.where(j <= 2 * low, both * (1 - 2 * ((2 * s) // S)), rest)
 
 
 def kernel(
     S, T, R, SL,
-    resid, pool, gmap, scale, oproj, gain, routes, routes_t, weight, wg, wu, wd,
+    resid, pool, gmap, scale, oproj, gain, routes_t, weight_t, wg, wu, wd,
     out,
     wgu_v, wd_v, opj, rim, piece, gout, stage, inbox, pbuf, rbuf, fbuf, fin, ret,
     acc, hid, mixed_v, normed_v,
@@ -103,16 +106,15 @@
     slot_row = rank_row + (e_row * SL).astype(F32)
     tgt_row = [jnp.sum(jnp.where(h, slot_row, 0.0), axis=0, keepdims=True) for h in hot_row]
 
-    EL = 128
-    e_col = lax.broadcasted_iota(jnp.int32, (R, EL), 1)
-    hot_col = [e_col == routes[:, k : k + 1] for k in range(2)]
-    both_col = jnp.where(hot_col[0] | hot_col[1], 1.0, 0.0).astype(BF)
-    after = lax.broadcasted_iota(jnp.int32, (R, R), 1) < lax.broadcasted_iota(
-        jnp.int32, (R, R), 0
-    )
-    rank_col = jnp.dot(jnp.where(after, 1.0, 0.0).astype(BF), both_col, preferred_element_type=F32)
-    slot_col = rank_col + (e_col * SL).astype(F32)
-    tgt_col = [jnp.sum(jnp.where(h, slot_col, 0.0), axis=1, keepdims=True) for h in hot_col]
+    eye = lax.broadcasted_iota(jnp.int32, (R, R), 0) == lax.broadcasted_iota(
+        jnp.int32, (R, R), 1
+    )
+
+    def column(row):
+        return jnp.sum(jnp.where(eye, row, 0.0), axis=1, keepdims=True)
+
+    tgt_col = [column(row) for row in tgt_row]
+    weight_col = [column(weight_t[k : k + 1, :]) for k in range(2)]
 
     rim_copy.wait_recv()
     values = pool[...].astype(F32)
@@ -158,7 +160,7 @@
     mixed_v[...] = mixed
     residual = mixed.astype(F32)
     scaled = residual * lax.rsqrt(jnp.mean(residual * residual, axis=1, keepdims=True) + norm_eps)
-    normed_v[...] = (scaled * gain[...].astype(F32)).astype(BF)
+    normed_v[...] = (scaled * gain[...].astype(F32).reshape(1, D)).astype(BF)
 
     slot_iota = lax.broadcasted_iota(jnp.int32, (SL, R), 0)
 
@@ -168,13 +170,16 @@
         return jnp.dot(place, normed_v[...], preferred_element_type=F32).astype(BF)
 
     def dest(j):
-        return lax.rem(s + offset(j) + S, S)
+        return nearest(s, S - j, S)
 
     def source(j):
-        return lax.rem(s - offset(j) + S, S)
-
-    def z_copy(j):
-        return remote(stage.at[j], inbox.at[s, t], z_s.at[j], z_r.at[j], sp=dest(j))
+        return nearest(s, lax.rem(S - j, S), S)
+
+    def z_copy(e):
+        return remote(stage.at[e], inbox.at[s, t], z_s.at[e], z_r.at[s], sp=e)
+
+    def z_arrival(i):
+        return remote(stage.at[i], inbox.at[i, t], z_s.at[i], z_r.at[i], sp=i)
 
     def far_copy(j, k):
         block = inbox.at[source(j), t]
@@ -199,34 +204,36 @@
         return remote(pbuf.at[j, q], fbuf.at[j, k], pf_s.at[j, k], pf_r.at[j, k], tp=q)
 
     def back(j):
-        return remote(fin.at[j], ret.at[s], rz_s.at[j], rz_r.at[j], sp=source(j))
+        return remote(fin.at[j], ret.at[s], rz_s.at[j], rz_r.at[s], sp=source(j))
+
+    def back_arrival(j):
+        e = source(j)
+        return remote(fin.at[j], ret.at[e], rz_s.at[j], rz_r.at[e], sp=e)
 
     inbox[s, t] = rows_of(s)
     forward_own(0)
 
     @pl.loop(1, S)
     def _(j):
-        stage[j] = rows_of(dest(j))
-        z_copy(j).start()
+        e = dest(j)
+        stage[e] = rows_of(e)
+        z_copy(e).start()
 
     for load in loads:
         load.wait()
 
     def arrive(j):
-        z_copy(j).wait_recv()
+        z_arrival(source(j)).wait_recv()
         forward_own(j)
-
-    if S > 1:
-        arrive(1)
 
     NT = 256 if (2 * F) % 256 == 0 else 128
     DT = 256 if D % 256 == 0 else 128
 
     @pl.loop(0, S + 2)
     def _(j):
-        @pl.when(j + 2 < S)
-        def _():
-            arrive(j + 2)
+        @pl.when((j + 1 < S) & (j + 1 > 0))
+        def _():
+            arrive(j + 1)
 
         @pl.when((j >= 1) & (j <= S))
         def _():
@@ -283,14 +290,14 @@
 
     @pl.loop(1, S)
     def _(j):
-        back(j).wait_recv()
+        back_arrival(j).wait_recv()
 
     ret[s] = fin[0]
     flat = ret[...].reshape(S * SL, D)
     lanes = lax.broadcasted_iota(jnp.int32, (R, S * SL), 1).astype(F32)
     total = mixed_v[...].astype(F32)
     picked = [
-        weight[:, k : k + 1]
+        weight_col[k]
         * jnp.dot(
             jnp.where(tgt_col[k] == lanes, 1.0, 0.0).astype(BF), flat, preferred_element_type=F32
         )
@@ -317,7 +324,7 @@
 
     @pl.loop(1, S)
     def _(j):
-        z_copy(j).wait_send()
+        z_copy(dest(j)).wait_send()
         back(j).wait_send()
 
 
@@ -340,7 +347,7 @@
     return pl.pallas_call(
         functools.partial(kernel, S, T, R, SL),
         out_shape=jax.ShapeDtypeStruct((R, D), BF),
-        in_specs=[vmem] * 9 + [hbm] * 3,
+        in_specs=[vmem] * 8 + [hbm] * 3,
         out_specs=vmem,
         scratch_shapes=[
             buf(D, 2 * F), buf(F, D), buf(T, GD, D), buf(RIM, GD), buf(T, R, GD), buf(T, R, GD),
@@ -356,7 +363,7 @@
         ),
     )(
         resid, pool_input, group_map, pool_scale.reshape(1, -1), out_proj,
-        norm_gain.reshape(1, -1), routes, routes.T, route_weight,
+        norm_gain, routes.T, route_weight.T,
         expert_gate[0], expert_up[0], expert_down[0],
     )
 

time: 120 us -> 108 us (0.900)
  the two profiles are of different devices: /device:TPU:0 before, /device:TPU:11 now
where the time goes in v2:
time: 108 us
  Pallas kernels  106 us (98%)
  local copies, waits for them, and re-layouts  1.88 us (2%)
    pallas_call x1, Pallas kernels, local(): pl.pallas_call(functools.partial(kernel, S, T, R, SL), out_shape=jax.Shap...  106 us

profile of v2, /device:TPU:11, one launch (start us, length us, event | category | flops | bytes accessed | tf_op | source)
XLA Modules:
  0.0 107.7 jit_solution(13733379328624502053)
XLA Ops:
  0.0 105.8 %shard_map.109 = bf16[128,2048]{1,0:T(8,128)(2,1)} custom-call(bf16[128,2048]{1,0:T(8,128)(2,1)} %resid.1, bf16[512,128]{1,0:T(8,128)(2,1)} %pool.1, bf16[1,128,128]{2,1,0:T(8,128)(2,1)} %gmap.1, bf16[1,128]{1,0:T(2,128)(2,1)} %bitcast.11, bf16[128,2048]{1,0:T(8,128)(2,1)} %oproj.1, bf16[2048]{0:T(1024)(128)(2,1)} %gain.1, s32[2,128]{1,0:T(2,128)} %bitcast.9, ...), custom_call_target="tpu_custom_call" | custom-call | tf_op jit(solution)/shard_map/pallas_call | solution.py:347
  105.8 1.9 %copy.13 = bf16[128,2048]{1,0:T(8,128)(2,1)} copy(bf16[128,2048]{1,0:T(8,128)(2,1)} %shard_map.109) | data formatting | bytes 1048576
